TPU v7x, 32 devices: a whole 2x2x4 slice. The times are simulated.
32 devices in a mesh: sp: 16 (over z, y, x), tp: 2 (over core).
Axes of the slice: x: 2, y: 2, z: 4, core: 2. Of those that a mesh axis runs over, the one named last changes fastest.
Arguments:
- residual_in: bfloat16 [4096, 2048], P(('sp', 'tp')), may hold values from -6 to 6
- query_lean: bfloat16 [4096, 8, 96], P('sp', 'tp'), may hold values from -60 to 60
- query_broad: bfloat16 [4096, 8, 160], P('sp', 'tp'), may hold values from -60 to 60
- latent: bfloat16 [4096, 256], P('sp'), may hold values from -6 to 6
- rope_key: bfloat16 [4096, 32], P('sp'), may hold values from -8 to 8
- latent_gain: float32 [256], replicated, may hold values from 0.1 to 1.9
- key_up_lean: bfloat16 [256, 8, 64], P(None, 'tp'), may hold values from -0.375 to 0.375
- key_up_broad: bfloat16 [256, 8, 128], P(None, 'tp'), may hold values from -0.375 to 0.375
- value_up_lean: bfloat16 [256, 8, 64], P(None, 'tp'), may hold values from -0.375 to 0.375
- value_up_broad: bfloat16 [256, 8, 128], P(None, 'tp'), may hold values from -0.375 to 0.375
- out_lean: bfloat16 [8, 64, 2048], P('tp'), may hold values from -0.15625 to 0.15625
- out_broad: bfloat16 [8, 128, 2048], P('tp'), may hold values from -0.15625 to 0.15625
- attn_gain: float32 [2048], replicated, may hold values from 0.1 to 1.9
- mlp_gain: float32 [2048], replicated, may hold values from 0.1 to 1.9
- gate_weight: bfloat16 [2048, 2816], P('sp', 'tp'), may hold values from -0.125 to 0.125
- up_weight: bfloat16 [2048, 2816], P('sp', 'tp'), may hold values from -0.125 to 0.125
- down_weight: bfloat16 [2816, 2048], P('tp', 'sp'), may hold values from -0.109375 to 0.109375
Outputs:
- layer_out: bfloat16 [4096, 2048], P(('sp', 'tp'))
All inputs are finite; a program needn't handle non-finite values.
Results may differ from a plain program's by a relative error of at most 0.015.
Values may be sent and summed in bfloat16 or wider, within the bound.
A program may use at most 128 MiB of HBM per device.

v0:
```python
import math
import jax
import jax.numpy as jnp
from jax import lax
from jax.sharding import PartitionSpec as P

THETA = 10000.0
EPS = 1e-06
NEGATIVE = -1e30


def rotate(values, positions):
    width = values.shape[-1]
    half = width // 2
    freqs = THETA ** (-2.0 * jnp.arange(half, dtype=jnp.float32) / width)
    angle = positions.astype(jnp.float32)[:, None] * freqs[None, :]
    cosine = jnp.cos(angle)
    sine = jnp.sin(angle)
    if values.ndim == 3:
        cosine = cosine[:, None, :]
        sine = sine[:, None, :]
    first = values[..., :half]
    second = values[..., half:]
    return jnp.concatenate(
        [first * cosine - second * sine, first * sine + second * cosine], axis=-1
    )


def normalize(values, gain):
    return values * lax.rsqrt(jnp.mean(values * values, axis=-1, keepdims=True) + EPS) * gain


def block_keys(weights, latent_rows):
    projected = []
    for key_up, value_up in weights:
        keys = jnp.einsum(
            "kr,rhd->khd", latent_rows, key_up, preferred_element_type=jnp.float32
        ).astype(jnp.bfloat16)
        values = jnp.einsum(
            "kr,rhd->khd", latent_rows, value_up, preferred_element_type=jnp.float32
        ).astype(jnp.bfloat16)
        projected.append((keys, values))
    return projected


def attend(carry, queries, projected, rotated_rows, key_pos, query_pos):
    updated = []
    visible = key_pos[None, :] <= query_pos[:, None]
    for state, query, pair in zip(carry, queries, projected):
        query_nope, query_rot, scale = query
        keys, values = pair
        peak, total, accum = state
        scores = (
            jnp.einsum("qhd,khd->hqk", query_nope, keys, preferred_element_type=jnp.float32)
            + jnp.einsum("qhr,kr->hqk", query_rot, rotated_rows, preferred_element_type=jnp.float32)
        ) * scale
        scores = jnp.where(visible[None], scores, NEGATIVE)
        new_peak = jnp.maximum(peak, jnp.max(scores, axis=-1))
        weights = jnp.where(visible[None], jnp.exp(scores - new_peak[..., None]), 0.0)
        factor = jnp.exp(peak - new_peak)
        total = total * factor + jnp.sum(weights, axis=-1)
        accum = accum * factor[..., None] + jnp.einsum(
            "hqk,khv->hqv", weights.astype(jnp.bfloat16), values, preferred_element_type=jnp.float32
        )
        updated.append((new_peak, total, accum))
    return tuple(updated)


def fold_piece(carry, latent_piece, rotated_piece, piece_pos, weights, segments):
    count = latent_piece.shape[0]
    block = math.gcd(count, 1024)
    last_all = segments[0][1][-1]

    def one_block(index, state):
        lat_rows = lax.dynamic_slice_in_dim(latent_piece, index * block, block, 0)
        rot_rows = lax.dynamic_slice_in_dim(rotated_piece, index * block, block, 0)
        pos_rows = lax.dynamic_slice_in_dim(piece_pos, index * block, block, 0)
        first_key = jnp.min(pos_rows)

        def work(inner):
            projected = block_keys(weights, lat_rows)
            results = []
            for inner_seg, segment in zip(inner, segments):
                queries, seg_pos = segment
                results.append(
                    lax.cond(
                        first_key <= seg_pos[-1],
                        lambda held, queries=queries, seg_pos=seg_pos: attend(
                            held, queries, projected, rot_rows, pos_rows, seg_pos
                        ),
                        lambda held: held,
                        inner_seg,
                    )
                )
            return tuple(results)

        return lax.cond(first_key <= last_all, work, lambda inner: inner, state)

    return lax.fori_loop(0, count // block, one_block, carry)


def shards(
    residual_in,
    query_lean,
    query_broad,
    latent,
    rope_key,
    latent_gain,
    key_up_lean,
    key_up_broad,
    value_up_lean,
    value_up_broad,
    out_lean,
    out_broad,
    attn_gain,
    mlp_gain,
    gate_weight,
    up_weight,
    down_weight,
):
    tokens_here = query_lean.shape[0]
    n_tp = lax.axis_size("tp")
    share = tokens_here // n_tp
    sp_index = lax.axis_index("sp")
    first = sp_index * tokens_here
    query_pos = first + jnp.arange(tokens_here, dtype=jnp.int32)
    rope_width = rope_key.shape[1]
    weights = ((key_up_lean, value_up_lean), (key_up_broad, value_up_broad))
    segment_rows = (query_lean, query_broad, query_pos)
    segments = []
    initial = []
    lean_rows, broad_rows, seg_pos = segment_rows
    queries = []
    states = []
    for query, value_up in ((lean_rows, value_up_lean), (broad_rows, value_up_broad)):
        nope = query.shape[2] - rope_width
        query_rot = rotate(query[:, :, nope:].astype(jnp.float32), seg_pos).astype(jnp.bfloat16)
        queries.append((query[:, :, :nope], query_rot, query.shape[2] ** (-0.5)))
        heads = query.shape[1]
        rows = query.shape[0]
        states.append(
            (
                jnp.full((heads, rows), NEGATIVE, jnp.float32),
                jnp.zeros((heads, rows), jnp.float32),
                jnp.zeros((heads, rows, value_up.shape[2]), jnp.float32),
            )
        )
    segments.append((tuple(queries), seg_pos))
    initial.append(tuple(states))
    segments = tuple(segments)
    initial = tuple(initial)
    sent_latent = normalize(latent.astype(jnp.float32), latent_gain).astype(jnp.bfloat16)
    sent_rot = rotate(rope_key.astype(jnp.float32), query_pos).astype(jnp.bfloat16)
    pieces = (
        lax.all_gather(sent_latent, "sp", axis=0, tiled=True),
        lax.all_gather(sent_rot, "sp", axis=0, tiled=True),
    )
    piece_pos = jnp.arange(pieces[0].shape[0], dtype=jnp.int32)
    folded = fold_piece(initial, pieces[0], pieces[1], piece_pos, weights, segments)
    results = [
        [(accum / total[..., None]).astype(jnp.bfloat16) for peak, total, accum in seg_state]
        for seg_state in folded
    ]
    attended = results[0]
    term = jnp.zeros((share * lax.axis_size("tp"), out_lean.shape[2]), jnp.float32)
    for rows_all, weight in ((attended[0], out_lean), (attended[1], out_broad)):
        rows = rows_all
        term = term + jnp.einsum("hqv,hvd->qd", rows, weight, preferred_element_type=jnp.float32)
    head_sum = lax.psum_scatter(
        term.astype(jnp.bfloat16), "tp", scatter_dimension=0, tiled=True
    ).astype(jnp.float32)
    branch = normalize(head_sum, attn_gain)
    kept = (residual_in.astype(jnp.float32) + branch).astype(jnp.bfloat16)
    normed = normalize(kept.astype(jnp.float32), mlp_gain).astype(jnp.bfloat16)
    whole_normed = lax.all_gather(normed, "tp", axis=0, tiled=True)
    gate_whole, up_whole, down_whole = (
        lax.all_gather(gate_weight, "sp", axis=0, tiled=True),
        lax.all_gather(up_weight, "sp", axis=0, tiled=True),
        lax.all_gather(down_weight, "sp", axis=1, tiled=True),
    )
    gate = jnp.dot(whole_normed, gate_whole, preferred_element_type=jnp.float32)
    up = jnp.dot(whole_normed, up_whole, preferred_element_type=jnp.float32)
    hidden = (jax.nn.silu(gate) * up).astype(jnp.bfloat16)
    rows = hidden
    channel_sum = lax.psum_scatter(
        jnp.dot(rows, down_whole, preferred_element_type=jnp.float32).astype(jnp.bfloat16),
        "tp",
        scatter_dimension=0,
        tiled=True,
    ).astype(jnp.float32)
    return (kept.astype(jnp.float32) + 0.5 * channel_sum).astype(jnp.bfloat16)


def solution(mesh):
    in_specs = (
        P(("sp", "tp"), None),
        P("sp", "tp", None),
        P("sp", "tp", None),
        P("sp", None),
        P("sp", None),
        P(),
        P(None, "tp", None),
        P(None, "tp", None),
        P(None, "tp", None),
        P(None, "tp", None),
        P("tp", None, None),
        P("tp", None, None),
        P(),
        P(),
        P("sp", "tp"),
        P("sp", "tp"),
        P("tp", "sp"),
    )
    out_specs = P(("sp", "tp"), None)
    return jax.shard_map(shards, mesh=mesh, in_specs=in_specs, out_specs=out_specs, check_vma=False)
```

profile of v0, /device:TPU:0, one launch (start us, length us, event | category | flops | bytes accessed | tf_op | source)
XLA Modules:
  0.0 533.8 jit_solution(12831282787911574293)
XLA Ops:
  7.7 1.7 fusion.59
  13.7 1.7 copy.22
  18.7 47.5 %all_gather.19 = bf16[4096,32]{0,1:T(8,128)(2,1)} all-gather(bf16[256,32]{0,1:T(8,128)(2,1)S(1)} %pad_maximum_fusion.2), channel_id=1, replica_groups=mesh['sp'=16,'tp'=2] {'sp'}, dimensions={0}, use_global_device_ids=true | all-gather | bytes 278528 | tf_op jit(solution)/shard_map/all_gather | solution.py:156
  66.2 8.1 %all-gather.6.cloned.1.call-done = bf16[4096,256]{1,0:T(8,128)(2,1)} async-done(((bf16[256,256]{1,0:T(8,128)(2,1)}), bf16[4096,256]{1,0:T(8,128)(2,1)}) %all-gather.6.cloned.1.call-update) | async-done | bytes 2097168 | tf_op jit(solution)/shard_map/all_gather | solution.py:155
  77.0 38.2 %while.24 = (s32[]{:T(128)}, f32[4,256]{1,0:T(4,128)S(1)}, f32[4,256]{1,0:T(4,128)S(1)}, f32[4,256,64]{1,2,0:T(8,128)}, f32[4,256]{1,0:T(4,128)S(1)}, /*index=5*...) while((s32[]{:T(128)}, f32[4,256]{1,0:T(4,128)S(1)}, ...), condition=%wide.region_11.12_spmd.clone, body=%wide.region_1.11_spmd.clone.sunk | while | flops 1768035584 | bytes 76572688 | solution.py:99
  77.0 1.4 fusion.91
  80.2 25.2 %conditional.4 = ((f32[4,256]{1,0:T(4,128)S(1)}, f32[4,256]{1,0:T(4,128)S(1)}, f32[4,256,64]{1,2,0:T(8,128)}, f32[4,256]{1,0:T(4,128)S(1)}, f32[4,256]{1,0:T(4,128)}, /*index=5*/f32[4,256,128]{2,1,0:T(8,128)})) conditional(s32[]{:T(128)} %convert_element_type.184, (f32[4,256]{1,0:T(4,128)S(1)}, f32[4,256]{1,0:T(4,128)S(1)}, f32[4,256,64]{1,2,0:T(8,128)}, ...), branch_computations={%region_3.0_spmd, %region_4.10_spmd} | conditional | flops 1768034560 | bytes 76562976 | solution.py:97
  80.2 1.5 fusion.40
  82.6 1.4 fusion.38
  84.9 2.4 convolution_convert_fusion
  90.3 15.1 %conditional = ((f32[4,256]{1,0:T(4,128)S(1)}, f32[4,256]{1,0:T(4,128)S(1)}, f32[4,256,64]{1,2,0:T(8,128)}, f32[4,256]{1,0:T(4,128)S(1)}, f32[4,256]{1,0:T(4,128)}, /*index=5*/f32[4,256,128]{2,1,0:T(8,128)})) conditional(s32[]{:T(128)} %convert_element_type.80, (f32[4,256]{1,0:T(4,128)S(1)}, f32[4,256]{1,0:T(4,128)S(1)}, f32[4,256,64]{1,2,0:T(8,128)}, ...), branch_computations={%region_5.0_spmd, %region_6.9_spmd} | conditional | flops 961155072 | bytes 57939176 | solution.py:86
  91.3 1.8 fusion.68
  93.1 1.3 fusion.66
  96.5 2.0 fusion.9
  98.6 1.3 multiply_add_fusion
  99.9 2.9 fusion.20
  102.8 2.6 fusion.23
  105.4 1.4 fusion.91
  108.7 1.4 fusion.91
  111.9 1.4 fusion.91
  115.2 1.9 convolution_bitcast_fusion.1
  117.2 2.5 fusion.48
  119.7 82.8 %reduce-scatter.3.cloned.1.call-done = bf16[128,2048]{1,0:T(8,128)(2,1)} async-done(((bf16[256,2048]{1,0:T(8,128)(2,1)}), bf16[128,2048]{1,0:T(8,128)(2,1)}) %reduce-scatter.3.cloned.1.call-update) | async-done | bytes 524304 | tf_op jit(solution)/shard_map/reduce_scatter | solution.py:169
  203.8 1.4 fusion.53
  208.2 8.4 %all-gather.8.cloned.1.call-done = bf16[256,2048]{1,0:T(8,128)(2,1)} async-done(((bf16[128,2048]{1,0:T(8,128)(2,1)}), bf16[256,2048]{1,0:T(8,128)(2,1)}) %all-gather.8.cloned.1.call-update) | async-done | bytes 1048592 | tf_op jit(solution)/shard_map/all_gather | solution.py:175
  216.6 92.5 %all-gather.10.cloned.1.call-done = bf16[2048,1408]{1,0:T(8,128)(2,1)} async-done(((bf16[128,1408]{1,0:T(8,128)(2,1)}), bf16[2048,1408]{1,0:T(8,128)(2,1)}) %all-gather.10.cloned.1.call-update) | async-done | bytes 5767184 | tf_op jit(solution)/shard_map/all_gather | solution.py:177
  309.1 5.9 %fusion.70 = f32[256,1408]{1,0:T(8,128)} fusion(bf16[256,2048]{1,0:T(8,128)(2,1)} %all-gather.8.cloned.1.call-done, bf16[2048,1408]{1,0:T(8,128)(2,1)} %all-gather.10.cloned.1.call-done), kind=kOutput, calls=%fused_computation.105 | convolution fusion | flops 1476395008 | bytes 8257536 | tf_op jit(solution)/shard_map/dot_general | solution.py:181
  315.0 84.1 %all-gather.12.cloned.1.call-done = bf16[2048,1408]{1,0:T(8,128)(2,1)} async-done(((bf16[128,1408]{1,0:T(8,128)(2,1)}), bf16[2048,1408]{1,0:T(8,128)(2,1)}) %all-gather.12.cloned.1.call-update) | async-done | bytes 5767184 | tf_op jit(solution)/shard_map/all_gather | solution.py:178
  399.1 109.6 %all-gather.14.cloned.1.call-done = bf16[1408,2048]{1,0:T(8,128)(2,1)} async-done(((bf16[1408,128]{1,0:T(8,128)(2,1)}), bf16[1408,2048]{1,0:T(8,128)(2,1)}) %all-gather.14.cloned.1.call-update) | async-done | bytes 5767184 | tf_op jit(solution)/shard_map/all_gather | solution.py:179
  508.7 9.5 %convolution_convert_fusion.2 = bf16[256,2048]{1,0:T(8,128)(2,1)} fusion(bf16[1408,2048]{1,0:T(8,128)(2,1)} %all-gather.14.cloned.1.call-done, bf16[256,2048]{1,0:T(8,128)(2,1)} %all-gather.8.cloned.1.call-done, bf16[2048,1408]{1,0:T(8,128)(2,1)} %all-gather.12.cloned.1.call-done, f32[256,1408]{1,0:T(8,128)} %fusion.70), kind=kOutput, calls=%fused_computation.57 | convolution fusion | flops 2955476992 | bytes 15073280 | tf_op jit(solution)/shard_map/dot_general | solution.py:186
  518.2 6.7 %reduce-scatter.5.cloned.1.call-done = bf16[128,2048]{1,0:T(8,128)(2,1)} async-done(((bf16[256,2048]{1,0:T(8,128)(2,1)}), bf16[128,2048]{1,0:T(8,128)(2,1)}) %reduce-scatter.5.cloned.1.call-update) | async-done | bytes 524304 | tf_op jit(solution)/shard_map/reduce_scatter | solution.py:185
  525.0 2.0 fusion.56
  (88 shorter events, 24.5 us)
Async XLA Ops:
  6.5 108.7 %copy-start = (bf16[4,128,2048]{2,1,0:T(8,128)(2,1)S(1)}, bf16[4,128,2048]{2,1,0:T(8,128)(2,1)}, u32[]{:S(2)}) copy-start(bf16[4,128,2048]{2,1,0:T(8,128)(2,1)} %param.34) | copy-start | bytes 6291460
  6.5 67.7 %all-gather.6.cloned.1.call-start = ((), (), s32[]{:S(2)}) async-start(), calls=%async_computation.2 | async-start | bytes 2228224 | tf_op jit(solution)/shard_map/all_gather | solution.py:155
  9.4 193.1 %reduce-scatter.3.cloned.1.call-start = ((), (), s32[]{:S(2)}) async-start(), calls=%async_computation.3 | async-start | bytes 1572864 | tf_op jit(solution)/shard_map/reduce_scatter | solution.py:169
  80.2 4.7 copy-start.1
  81.8 5.9 %copy-start.11 = (s32[256]{0:T(256)S(1)}, s32[256]{0:T(256)}, u32[]{:S(2)}) copy-start(s32[256]{0:T(256)} %get-tuple-element.684) | copy-start | bytes 3076 | tf_op jit(solution)/shard_map/while/body/eval_jaxpr/cond
  87.7 0.6 copy-start.10
  90.3 2.7 copy-start.5
  90.3 2.7 copy-start.6
  93.1 1.3 copy-start.4
  94.4 0.8 copy-start.7
  96.5 3.4 copy-start.2
  98.6 4.2 copy-start.3
  115.2 2.0 copy-start.8
  117.1 86.6 %copy-start.9 = (bf16[128,2048]{1,0:T(8,128)(2,1)S(1)}, bf16[128,2048]{1,0:T(8,128)(2,1)}, u32[]{:S(2)}) copy-start(bf16[128,2048]{1,0:T(8,128)(2,1)} %param.23) | copy-start | bytes 1572868
  117.1 86.6 %copy-start.12 = (f32[2048]{0:T(1024)S(1)}, f32[2048]{0:T(1024)}, u32[]{:S(2)}) copy-start(f32[2048]{0:T(1024)} %param.35) | copy-start | bytes 24580
  117.2 88.1 %copy-start.13 = (f32[2048]{0:T(1024)S(1)}, f32[2048]{0:T(1024)}, u32[]{:S(2)}) copy-start(f32[2048]{0:T(1024)} %param.36) | copy-start | bytes 24580
  119.7 96.9 %all-gather.8.cloned.1.call-start = ((), (), s32[]{:S(2)}) async-start(), calls=%async_computation.4 | async-start | bytes 1572864 | tf_op jit(solution)/shard_map/all_gather | solution.py:175
  206.2 102.9 %all-gather.10.cloned.1.call-start = ((), (), s32[]{:S(2)}) async-start(), calls=%async_computation.5 | async-start | bytes 6127616 | tf_op jit(solution)/shard_map/all_gather | solution.py:177
  206.8 192.3 %all-gather.12.cloned.1.call-start = ((), (), s32[]{:S(2)}) async-start(), calls=%async_computation.6 | async-start | bytes 6127616 | tf_op jit(solution)/shard_map/all_gather | solution.py:178
  207.4 301.3 %all-gather.14.cloned.1.call-start = ((), (), s32[]{:S(2)}) async-start(), calls=%async_computation.7 | async-start | bytes 6127616 | tf_op jit(solution)/shard_map/all_gather | solution.py:179
  208.0 317.0 %reduce-scatter.5.cloned.1.call-start = ((), (), s32[]{:S(2)}) async-start(), calls=%async_computation.8 | async-start | bytes 1572864 | tf_op jit(solution)/shard_map/reduce_scatter | solution.py:185
Sparse Core Ops, SparseCore 0:
  10.1 64.0 all-gather.5
  119.8 82.6 reduce-scatter.2
  206.4 10.2 all-gather.7
  219.2 89.9 all-gather.9
  311.7 87.4 all-gather.11
  401.7 106.9 all-gather.13
  518.4 6.5 reduce-scatter.4
where the time goes:
time: 536 us; the launch traced here: 534 us
  waiting for transfers between devices  394 us (74%)
  blocking collectives  47.5 us (9%)
  matrix products  36 us (7%)
  other arithmetic  23.2 us (4%)
  between operations  13.6 us (3%)
  local copies, waits for them, and re-layouts  12.5 us (2%)
  loops' own time  6.69 us (1%)
    all_gather x1, waiting for transfers between devices, shards(): lax.all_gather(down_weight, 'sp', axis=1, tiled=True)  110 us
    all_gather x1, waiting for transfers between devices, shards(): lax.all_gather(gate_weight, 'sp', axis=0, tiled=True)  92.5 us
    all_gather x1, waiting for transfers between devices, shards(): lax.all_gather(up_weight, 'sp', axis=0, tiled=True)  84.1 us
    reduce_scatter x1, waiting for transfers between devices, shards(): lax.psum_scatter(term.astype(jnp.bfloat16), 'tp', scatter_dimension=0, ti...  82.8 us
    all_gather x1, blocking collectives, shards(): lax.all_gather(sent_rot, 'sp', axis=0, tiled=True)  47.5 us
  transfers between devices with their start and end apart: 7, of which 7 were waited for; matrix products, arithmetic and copies ran while one was open for 3% of the time, Pallas kernels for 0%

commit v1 on v0

--- a/solution.py
+++ b/solution.py
@@ -176,7 +176,7 @@
     gate_whole, up_whole, down_whole = (
         lax.all_gather(gate_weight, "sp", axis=0, tiled=True),
         lax.all_gather(up_weight, "sp", axis=0, tiled=True),
-        lax.all_gather(down_weight, "sp", axis=1, tiled=True),
+        jnp.concatenate(lax.all_gather(down_weight, "sp"), axis=1),
     )
     gate = jnp.dot(whole_normed, gate_whole, preferred_element_type=jnp.float32)
     up = jnp.dot(whole_normed, up_whole, preferred_element_type=jnp.float32)

time: 536 us -> 514 us (0.959)
  waiting for transfers between devices: 394 us -> 364 us
  local copies, waits for them, and re-layouts: 12.5 us -> 20.8 us
    all_gather x1, waiting for transfers between devices: 110 us -> 87.6 us  [shards(): lax.all_gather(down_weight, 'sp')]
    reshape x0 -> x1, local copies, waits for them, and re-layouts: none -> 8.27 us  [shards(): jnp.concatenate(lax.all_gather(down_weight, 'sp'), axis=1)]
    all_gather x1, waiting for transfers between devices: 8.42 us -> 0.86 us  [shards(): whole_normed = lax.all_gather(normed, 'tp', axis=0, tiled=True)]
  transfers between devices with their start and end apart: 7 -> 7, of which waited for: 7 -> 7; matrix products, arithmetic and copies ran while one was open for 3% -> 5% of each run, Pallas kernels for 0% -> 0%
where the time goes in v1:
time: 514 us; the launch traced here: 512 us
  waiting for transfers between devices  364 us (71%)
  blocking collectives  47.5 us (9%)
  matrix products  36 us (7%)
  other arithmetic  23.2 us (5%)
  local copies, waits for them, and re-layouts  20.8 us (4%)
  between operations  13.6 us (3%)
  loops' own time  6.69 us (1%)
    all_gather x1, waiting for transfers between devices, shards(): lax.all_gather(gate_weight, 'sp', axis=0, tiled=True)  92.5 us
    all_gather x1, waiting for transfers between devices, shards(): lax.all_gather(down_weight, 'sp')  87.6 us
    all_gather x1, waiting for transfers between devices, shards(): lax.all_gather(up_weight, 'sp', axis=0, tiled=True)  84.1 us
    reduce_scatter x1, waiting for transfers between devices, shards(): lax.psum_scatter(term.astype(jnp.bfloat16), 'tp', scatter_dimension=0, ti...  82 us
    all_gather x1, blocking collectives, shards(): lax.all_gather(sent_rot, 'sp', axis=0, tiled=True)  47.5 us
  transfers between devices with their start and end apart: 7, of which 7 were waited for; matrix products, arithmetic and copies ran while one was open for 5% of the time, Pallas kernels for 0%

profile of v1, /device:TPU:0, one launch (start us, length us, event | category | flops | bytes accessed | tf_op | source)
XLA Modules:
  0.0 512.4 jit_solution(2298064215357424612)
XLA Ops:
  7.7 1.7 fusion.59
  13.7 1.7 copy.32
  18.7 47.5 %all_gather.22 = bf16[4096,32]{0,1:T(8,128)(2,1)} all-gather(bf16[256,32]{0,1:T(8,128)(2,1)S(1)} %pad_maximum_fusion.2), channel_id=1, replica_groups=mesh['sp'=16,'tp'=2] {'sp'}, dimensions={0}, use_global_device_ids=true | all-gather | bytes 278528 | tf_op jit(solution)/shard_map/all_gather | solution.py:156
  66.2 8.1 %all-gather.7.cloned.1.call-done = bf16[4096,256]{1,0:T(8,128)(2,1)} async-done(((bf16[256,256]{1,0:T(8,128)(2,1)}), bf16[4096,256]{1,0:T(8,128)(2,1)}) %all-gather.7.cloned.1.call-update) | async-done | bytes 2097168 | tf_op jit(solution)/shard_map/all_gather | solution.py:155
  77.0 38.2 %while.24 = (s32[]{:T(128)}, f32[4,256]{1,0:T(4,128)S(1)}, f32[4,256]{1,0:T(4,128)S(1)}, f32[4,256,64]{1,2,0:T(8,128)}, f32[4,256]{1,0:T(4,128)S(1)}, /*index=5*...) while((s32[]{:T(128)}, f32[4,256]{1,0:T(4,128)S(1)}, ...), condition=%wide.region_11.12_spmd.clone, body=%wide.region_1.11_spmd.clone.sunk | while | flops 1768035584 | bytes 76572688 | solution.py:99
  77.0 1.4 fusion.91
  80.2 25.2 %conditional.4 = ((f32[4,256]{1,0:T(4,128)S(1)}, f32[4,256]{1,0:T(4,128)S(1)}, f32[4,256,64]{1,2,0:T(8,128)}, f32[4,256]{1,0:T(4,128)S(1)}, f32[4,256]{1,0:T(4,128)}, /*index=5*/f32[4,256,128]{2,1,0:T(8,128)})) conditional(s32[]{:T(128)} %convert_element_type.184, (f32[4,256]{1,0:T(4,128)S(1)}, f32[4,256]{1,0:T(4,128)S(1)}, f32[4,256,64]{1,2,0:T(8,128)}, ...), branch_computations={%region_3.0_spmd, %region_4.10_spmd} | conditional | flops 1768034560 | bytes 76562976 | solution.py:97
  80.2 1.5 fusion.40
  82.6 1.4 fusion.38
  84.9 2.4 convolution_convert_fusion
  90.3 15.1 %conditional = ((f32[4,256]{1,0:T(4,128)S(1)}, f32[4,256]{1,0:T(4,128)S(1)}, f32[4,256,64]{1,2,0:T(8,128)}, f32[4,256]{1,0:T(4,128)S(1)}, f32[4,256]{1,0:T(4,128)}, /*index=5*/f32[4,256,128]{2,1,0:T(8,128)})) conditional(s32[]{:T(128)} %convert_element_type.80, (f32[4,256]{1,0:T(4,128)S(1)}, f32[4,256]{1,0:T(4,128)S(1)}, f32[4,256,64]{1,2,0:T(8,128)}, ...), branch_computations={%region_5.0_spmd, %region_6.9_spmd} | conditional | flops 961155072 | bytes 57939176 | solution.py:86
  91.3 1.8 fusion.68
  93.1 1.3 fusion.66
  96.5 2.0 fusion.9
  98.6 1.3 multiply_add_fusion
  99.9 2.9 fusion.20
  102.8 2.6 fusion.23
  105.4 1.4 fusion.91
  108.7 1.4 fusion.91
  111.9 1.4 fusion.91
  115.2 1.9 convolution_bitcast_fusion.1
  117.2 2.5 fusion.48
  120.5 82.0 %reduce-scatter.3.cloned.1.call-done = bf16[128,2048]{1,0:T(8,128)(2,1)} async-done(((bf16[256,2048]{1,0:T(8,128)(2,1)}), bf16[128,2048]{1,0:T(8,128)(2,1)}) %reduce-scatter.3.cloned.1.call-update) | async-done | bytes 524304 | tf_op jit(solution)/shard_map/reduce_scatter | solution.py:169
  203.8 1.4 fusion.53
  207.6 87.6 %all-gather.15.cloned.1.call-done = bf16[22528,128]{1,0:T(8,128)(2,1)} async-done(((bf16[1408,128]{1,0:T(8,128)(2,1)}), bf16[22528,128]{1,0:T(8,128)(2,1)}) %all-gather.15.cloned.1.call-update) | async-done | bytes 5767184 | tf_op jit(solution)/shard_map/all_gather | solution.py:179
  295.2 8.3 %copy.33 = bf16[1408,16,128]{0,2,1:T(8,128)(2,1)} copy(bf16[1408,16,128]{2,0,1:T(8,128)(2,1)} %bitcast.65) | data formatting | bytes 11534336 | tf_op jit(solution)/shard_map/reshape | solution.py:179
  304.3 92.5 %all-gather.11.cloned.1.call-done = bf16[2048,1408]{1,0:T(8,128)(2,1)} async-done(((bf16[128,1408]{1,0:T(8,128)(2,1)}), bf16[2048,1408]{1,0:T(8,128)(2,1)}) %all-gather.11.cloned.1.call-update) | async-done | bytes 5767184 | tf_op jit(solution)/shard_map/all_gather | solution.py:177
  396.8 5.9 %fusion.70 = f32[256,1408]{1,0:T(8,128)} fusion(bf16[256,2048]{1,0:T(8,128)(2,1)} %all-gather.9.cloned.1.call-done, bf16[2048,1408]{1,0:T(8,128)(2,1)} %all-gather.11.cloned.1.call-done), kind=kOutput, calls=%fused_computation.105 | convolution fusion | flops 1476395008 | bytes 8257536 | tf_op jit(solution)/shard_map/dot_general | solution.py:181
  402.7 84.1 %all-gather.13.cloned.1.call-done = bf16[2048,1408]{1,0:T(8,128)(2,1)} async-done(((bf16[128,1408]{1,0:T(8,128)(2,1)}), bf16[2048,1408]{1,0:T(8,128)(2,1)}) %all-gather.13.cloned.1.call-update) | async-done | bytes 5767184 | tf_op jit(solution)/shard_map/all_gather | solution.py:178
  486.8 9.5 %convolution_convert_fusion.2 = bf16[256,2048]{1,0:T(8,128)(2,1)} fusion(bf16[1408,2048]{0,1:T(8,128)(2,1)} %bitcast.66, bf16[256,2048]{1,0:T(8,128)(2,1)} %all-gather.9.cloned.1.call-done, bf16[2048,1408]{1,0:T(8,128)(2,1)} %all-gather.13.cloned.1.call-done, f32[256,1408]{1,0:T(8,128)} %fusion.70), kind=kOutput, calls=%fused_computation.57 | convolution fusion | flops 2955476992 | bytes 15073280 | tf_op jit(solution)/shard_map/dot_general | solution.py:186
  496.4 7.2 %reduce-scatter.5.cloned.1.call-done = bf16[128,2048]{1,0:T(8,128)(2,1)} async-done(((bf16[256,2048]{1,0:T(8,128)(2,1)}), bf16[128,2048]{1,0:T(8,128)(2,1)}) %reduce-scatter.5.cloned.1.call-update) | async-done | bytes 524304 | tf_op jit(solution)/shard_map/reduce_scatter | solution.py:185
  503.6 2.0 fusion.56
  (89 shorter events, 25.5 us)
Async XLA Ops:
  6.5 108.7 %copy-start = (bf16[4,128,2048]{2,1,0:T(8,128)(2,1)S(1)}, bf16[4,128,2048]{2,1,0:T(8,128)(2,1)}, u32[]{:S(2)}) copy-start(bf16[4,128,2048]{2,1,0:T(8,128)(2,1)} %param.34) | copy-start | bytes 6291460
  6.5 67.7 %all-gather.7.cloned.1.call-start = ((), (), s32[]{:S(2)}) async-start(), calls=%async_computation.2 | async-start | bytes 2228224 | tf_op jit(solution)/shard_map/all_gather | solution.py:155
  9.4 193.1 %reduce-scatter.3.cloned.1.call-start = ((), (), s32[]{:S(2)}) async-start(), calls=%async_computation.3 | async-start | bytes 1572864 | tf_op jit(solution)/shard_map/reduce_scatter | solution.py:169
  80.2 4.7 copy-start.1
  81.8 5.9 %copy-start.11 = (s32[256]{0:T(256)S(1)}, s32[256]{0:T(256)}, u32[]{:S(2)}) copy-start(s32[256]{0:T(256)} %get-tuple-element.724) | copy-start | bytes 3076 | tf_op jit(solution)/shard_map/while/body/eval_jaxpr/cond
  87.7 0.6 copy-start.10
  90.3 2.7 copy-start.5
  90.3 2.7 copy-start.6
  93.1 1.3 copy-start.4
  94.4 0.8 copy-start.7
  96.5 3.4 copy-start.2
  98.6 4.2 copy-start.3
  115.2 2.0 copy-start.8
  117.1 86.6 %copy-start.9 = (bf16[128,2048]{1,0:T(8,128)(2,1)S(1)}, bf16[128,2048]{1,0:T(8,128)(2,1)}, u32[]{:S(2)}) copy-start(bf16[128,2048]{1,0:T(8,128)(2,1)} %param.23) | copy-start | bytes 1572868
  117.1 86.6 %copy-start.12 = (f32[2048]{0:T(1024)S(1)}, f32[2048]{0:T(1024)}, u32[]{:S(2)}) copy-start(f32[2048]{0:T(1024)} %param.35) | copy-start | bytes 24580
  117.2 88.1 %copy-start.13 = (f32[2048]{0:T(1024)S(1)}, f32[2048]{0:T(1024)}, u32[]{:S(2)}) copy-start(f32[2048]{0:T(1024)} %param.36) | copy-start | bytes 24580
  119.7 175.5 %all-gather.15.cloned.1.call-start = ((), (), s32[]{:S(2)}) async-start(), calls=%async_computation.8 | async-start | bytes 6127616 | tf_op jit(solution)/shard_map/all_gather | solution.py:179
  120.4 183.9 %all-gather.9.cloned.1.call-start = ((), (), s32[]{:S(2)}) async-start(), calls=%async_computation.4 | async-start | bytes 1572864 | tf_op jit(solution)/shard_map/all_gather | solution.py:175
  206.2 190.6 %all-gather.11.cloned.1.call-start = ((), (), s32[]{:S(2)}) async-start(), calls=%async_computation.5 | async-start | bytes 6127616 | tf_op jit(solution)/shard_map/all_gather | solution.py:177
  206.8 280.0 %all-gather.13.cloned.1.call-start = ((), (), s32[]{:S(2)}) async-start(), calls=%async_computation.6 | async-start | bytes 6127616 | tf_op jit(solution)/shard_map/all_gather | solution.py:178
  207.4 296.2 %reduce-scatter.5.cloned.1.call-start = ((), (), s32[]{:S(2)}) async-start(), calls=%async_computation.7 | async-start | bytes 1572864 | tf_op jit(solution)/shard_map/reduce_scatter | solution.py:185
Sparse Core Ops, SparseCore 0:
  10.1 64.0 all-gather.6
  119.8 82.6 reduce-scatter.2
  205.2 89.9 all-gather.14
  296.6 7.6 all-gather.8
  306.9 89.9 all-gather.10
  399.4 87.4 all-gather.12
  496.5 7.0 reduce-scatter.4
